TPU v7x, 512 devices: a whole 4x4x16 slice. The times are simulated.
512 devices in a mesh: sp: 32 (over z, core), tp: 16 (over y, x).
Axes of the slice: x: 4, y: 4, z: 16, core: 2. Of those that a mesh axis runs over, the one named last changes fastest.
Arguments:
- query_heads: bfloat16 [8192, 1024], P('sp', 'tp'), may hold values from -6 to 6
- key_heads: bfloat16 [8192, 256], P('sp'), may hold values from -6 to 6
- value_heads: bfloat16 [8192, 256], P('sp'), may hold values from -24 to 24
- q_gain: float32 [64], replicated, may hold values from 0.6 to 4.5
- k_gain: float32 [64], replicated, may hold values from 0.6 to 4.5
- out_weight: bfloat16 [1024, 2048], P('tp'), may hold values from -0.1875 to 0.1875
- residual: bfloat16 [8192, 2048], P('sp', 'tp'), may hold values from -3 to 3
- norm_gain: float32 [2048], P('tp'), may hold values from 0.1 to 1.9
- routes: int32 [8192, 2], P('sp'), may hold values from 0 to 31, all different within a row; in each aligned block of 256 rows (0 to 255, 256 to 511, ...) at most 21 rows name the same one
- route_weights: float32 [8192, 2], P('sp'), may hold values from 0.5 to 1.5
- w_gate: bfloat16 [32, 2048, 4096], P('sp', None, 'tp'), may hold values from -0.125 to 0.125
- w_up: bfloat16 [32, 2048, 4096], P('sp', None, 'tp'), may hold values from -0.125 to 0.125
- w_down: bfloat16 [32, 4096, 2048], P('sp', 'tp'), may hold values from -0.1875 to 0.1875
Outputs:
- layer_out: bfloat16 [8192, 2048], P('sp', 'tp')
Inputs may be any that keep to these rules, and one draw needn't show every extreme that they name: `routes`: each row names 2 different experts. Among the 256 rows of one index of sp, no expert is named more than 21 times, a bound that some block reaches.
All inputs are finite; a program needn't handle non-finite values.
Results may differ from a plain program's by a relative error of at most 0.02.
The roundings to bfloat16 on the way count: a program that leaves them out, or rounds other values in their place, can miss the bound.
Values may be sent and summed in bfloat16 or wider, within the bound.
A program may use at most 64 MiB of HBM per device.

v0:
```python
import jax
import jax.numpy as jnp
from jax import lax
from jax.sharding import Mesh
from jax.sharding import PartitionSpec as P

D = 2048
HQ = 16
KV = 4
E = 64
TOPK = 2
GRID_W = 64
TP = ("tp_0", "tp_1")


norm_eps = 1e-06
rope_base = 10000.0


def side_by_side(arrays, axis, dim, along):
    ends, at = ([], 0)
    for a in arrays[:-1]:
        at += a.shape[along]
        ends.append(at)
    both = jnp.concatenate(arrays, axis=along)
    return tuple(jnp.split(lax.all_gather(both, axis, axis=dim, tiled=True), ends, axis=along))


def cut_along(array, dim, peers):
    dims = array.shape
    tiles = array.reshape(*dims[:dim], peers, dims[dim] // peers, *dims[dim + 1 :])
    return jnp.moveaxis(tiles, dim, 0)


def sum_at_owner(array, axis, dim):
    peers = lax.axis_size(axis)
    tiles = lax.all_to_all(cut_along(array, dim, peers), axis, 0, 0, tiled=True)
    return jnp.sum(tiles.astype(jnp.float32), axis=0)


def by_axis(array, axes):
    for axis in axes:
        array = lax.psum(array, axis)
    return array


def gather_axes(array, axes, dim):
    if not axes:
        return array
    nearer = lax.all_gather(array, axes[-1], axis=dim, tiled=True)
    return gather_axes(nearer, axes[:-1], dim)


def normalize(values_f, gain):
    mean_sq = jnp.mean(values_f * values_f, axis=-1, keepdims=True)
    return values_f * lax.rsqrt(mean_sq + norm_eps) * gain


def rotate(values_f, positions):
    head_width = values_f.shape[-1]
    half_width = head_width // 2
    quarter_width = half_width // 2
    frequency = rope_base ** (-jnp.arange(quarter_width, dtype=jnp.float32) / quarter_width)
    grid_rows = (positions // GRID_W).astype(jnp.float32)
    grid_cols = (positions % GRID_W).astype(jnp.float32)
    shape = (values_f.shape[0],) + (1,) * (values_f.ndim - 2) + (quarter_width,)
    pieces = []
    for coords, offset_lo in ((grid_rows, 0), (grid_cols, half_width)):
        angles = coords[:, None] * frequency[None, :]
        cosine = jnp.cos(angles).reshape(shape)
        sines = jnp.sin(angles).reshape(shape)
        first_part = values_f[..., offset_lo : offset_lo + quarter_width]
        second_part = values_f[..., offset_lo + quarter_width : offset_lo + half_width]
        pieces.append(first_part * cosine - second_part * sines)
        pieces.append(second_part * cosine + first_part * sines)
    return jnp.concatenate(pieces, axis=-1)


def shards(
    query_heads,
    key_heads,
    value_heads,
    q_gain,
    k_gain,
    out_weight,
    residual,
    norm_gain,
    routes,
    route_weights,
    w_gate,
    w_up,
    w_down,
):
    tok_rows = query_heads.shape[0]
    head_local = query_heads.shape[1] // E
    group_size = HQ // KV
    kv_count = max(head_local // group_size, 1)
    per_kv = head_local // kv_count
    tp_index = lax.axis_index(TP)
    sp_index = lax.axis_index("sp")
    kv_first = tp_index * head_local // group_size
    positions = sp_index * tok_rows + jnp.arange(tok_rows, dtype=jnp.int32)
    query_f = query_heads.astype(jnp.float32).reshape(tok_rows, kv_count, per_kv, E)
    q_turned = rotate(normalize(query_f, q_gain), positions).astype(jnp.bfloat16)
    key_cols = lax.dynamic_slice_in_dim(key_heads, kv_first * E, kv_count * E, 1)
    value_cols = lax.dynamic_slice_in_dim(value_heads, kv_first * E, kv_count * E, 1)
    key_f = key_cols.astype(jnp.float32).reshape(tok_rows, kv_count, E)
    k_turned = rotate(normalize(key_f, k_gain), positions).astype(jnp.bfloat16)
    value_sel = value_cols.reshape(tok_rows, kv_count, E)
    run_max = jnp.full((kv_count, per_kv, tok_rows), -1e30, jnp.float32)
    key_block, value_block = side_by_side((k_turned, value_sel), "sp", 0, 1)
    scores = jnp.einsum(
        "qcge,kce->cgqk", q_turned, key_block, preferred_element_type=jnp.float32
    ) * E ** (-0.5)
    new_max = jnp.maximum(run_max, jnp.max(scores, axis=-1))
    exped = jnp.exp(scores - new_max[..., None])
    denominator = jnp.sum(exped, axis=-1)
    weighted = jnp.einsum(
        "cgqk,kce->cgqe",
        exped.astype(jnp.bfloat16),
        value_block,
        preferred_element_type=jnp.float32,
    )
    run_max, denominator, weighted = (new_max, denominator, weighted)
    attended = (weighted / denominator[..., None]).astype(jnp.bfloat16)
    attended = attended.transpose(2, 0, 1, 3).reshape(tok_rows, head_local * E)
    partial_value = jnp.dot(attended, out_weight, preferred_element_type=jnp.float32).astype(
        jnp.bfloat16
    )
    attn_out = sum_at_owner(partial_value, TP, 1)
    after_attn = residual.astype(jnp.float32) + attn_out
    square_sum = by_axis(jnp.sum(after_attn * after_attn, axis=1), TP)
    normed = (after_attn * lax.rsqrt(square_sum / D + norm_eps)[:, None] * norm_gain).astype(
        jnp.bfloat16
    )
    experts_n = lax.axis_size("sp")
    capacity = 5 * tok_rows * TOPK // (4 * experts_n) + 1
    assign = routes.reshape(tok_rows * TOPK)
    onehot = (assign[:, None] == jnp.arange(experts_n, dtype=jnp.int32)[None, :]).astype(jnp.int32)
    before = jnp.cumsum(onehot, axis=0) - onehot
    slot_rank = jnp.sum(before * onehot, axis=1)
    slot_index = assign * capacity + slot_rank
    token_local = jnp.arange(tok_rows * TOPK, dtype=jnp.int32) // TOPK
    slot_token = (
        jnp.full((experts_n * capacity,), tok_rows, jnp.int32).at[slot_index].set(token_local)
    )
    gate_w = w_gate[0]
    up_w = w_up[0]
    down_w = w_down[0]
    padded = jnp.concatenate([normed, jnp.zeros((1, normed.shape[1]), jnp.bfloat16)], axis=0)
    slot_rows = padded[slot_token].reshape(experts_n, capacity, normed.shape[1])
    block_rows = gather_axes(
        lax.all_to_all(slot_rows, "sp", split_axis=0, concat_axis=0, tiled=True), TP, 2
    )
    gate_next = jnp.einsum("scd,df->scf", block_rows, gate_w, preferred_element_type=jnp.float32)
    up_next = jnp.einsum("scd,df->scf", block_rows, up_w, preferred_element_type=jnp.float32)
    activated = (jax.nn.silu(gate_next) * up_next).astype(jnp.bfloat16)
    partials = jnp.einsum(
        "scf,fd->scd", activated, down_w, preferred_element_type=jnp.float32
    ).astype(jnp.bfloat16)
    expert_rows = sum_at_owner(partials, TP, 2).astype(jnp.bfloat16)
    returned_rows = lax.all_to_all(expert_rows, "sp", split_axis=0, concat_axis=0, tiled=True)
    columns = returned_rows.shape[2]
    picked = returned_rows.reshape(experts_n * capacity, columns)[slot_index].astype(jnp.float32)
    picked = picked.reshape(tok_rows, TOPK, columns)
    expert_mix = jnp.sum(picked * route_weights[:, :, None], axis=1)
    return (after_attn + expert_mix).astype(jnp.bfloat16)


def solution(mesh):
    finer = Mesh(mesh.devices.reshape(mesh.shape["sp"], 4, 4), ("sp", "tp_0", "tp_1"))
    in_specs = (
        P("sp", TP),
        P("sp", None),
        P("sp", None),
        P(),
        P(),
        P(TP, None),
        P("sp", TP),
        P(TP),
        P("sp", None),
        P("sp", None),
        P("sp", None, TP),
        P("sp", None, TP),
        P("sp", TP, None),
    )
    out_specs = P("sp", TP)
    return jax.shard_map(
        shards, mesh=finer, in_specs=in_specs, out_specs=out_specs, check_vma=False
    )
```

profile of v0, /device:TPU:1, one launch (start us, length us, event | category | flops | bytes accessed | tf_op | source)
XLA Modules:
  0.0 319.0 jit_solution(1693130375576964140)
XLA Ops:
  10.6 1.2 reduce-window.6
  13.9 74.3 %all-gather.3.cloned.1.call-done = bf16[8192,2,64]{0,2,1:T(8,128)(2,1)} async-done(((bf16[256,2,64]{0,2,1:T(8,128)(2,1)}), bf16[8192,2,64]{0,2,1:T(8,128)(2,1)}) %all-gather.3.cloned.1.call-update) | async-done | bytes 2097168 | tf_op jit(solution)/shard_map/all_gather | solution.py:26
  88.2 2.8 fusion.90
  91.0 3.2 %copy-done.1 = f32[8192,256]{1,0:T(8,128)} copy-done((f32[8192,256]{1,0:T(8,128)}, f32[8192,256]{1,0:T(8,128)S(1)}, u32[]{:S(2)}) %copy-start.1) | copy-done | bytes 8388632
  94.2 1.2 fusion.1
  95.4 5.8 %fusion.8 = bf16[32,16,8,128]{3,2,1,0:T(8,128)(2,1)S(1)} fusion(bf16[64,2048]{1,0:T(8,128)(2,1)S(1)} %copy-done.3, f32[8192,256]{1,0:T(8,128)} %copy-done.1, f32[256]{0:T(256)S(1)} %broadcast_maximum_fusion, bf16[8192,2,64]{0,2,1:T(8,128)(2,1)} %all-gather.3.cloned.1.call-done, f32[256]{0:T(256)S(1)} %fusion.1), kind=kOutput, calls=%fused_computation.16 | convolution fusion | flops 340295680 | bytes 10749952 | tf_op jit(solution)/shard_map/dot_general | solution.py:127
  101.2 1.3 copy.62
  102.5 6.5 %all-to-all-start = ((bf16[16,256,128]{2,1,0:T(8,128)(2,1)}), bf16[16,256,128]{2,1,0:T(8,128)(2,1)S(1)}, u32[]{:S(2)}, u32[]{:S(2)}) async-start(bf16[16,256,128]{2,1,0:T(8,128)(2,1)} %bitcast.106), calls=%async_computation | async-start | bytes 2097152 | tf_op jit(solution)/shard_map/all_to_all | solution.py:37
  109.5 2.4 scatter_custom_fusion
  112.0 13.5 %all-to-all-done = bf16[16,256,128]{2,1,0:T(8,128)(2,1)S(1)} async-done(((bf16[16,256,128]{2,1,0:T(8,128)(2,1)}), bf16[16,256,128]{2,1,0:T(8,128)(2,1)S(1)}, u32[]{:S(2)}, u32[]{:S(2)}) %all-to-all-start) | async-done | bytes 1048608 | tf_op jit(solution)/shard_map/all_to_all | solution.py:37
  125.7 6.6 %psum.14 = f32[256]{0:T(256)S(1)} all-reduce(f32[256]{0:T(256)S(1)} %multiply_reduce_fusion), channel_id=1, replica_groups=mesh['sp'=32,'tp_0'=4,'tp_1'=4] {'tp_0'}, use_global_device_ids=true, to_apply=%region_6.7 | all-reduce | flops 256 | bytes 2048 | tf_op jit(solution)/shard_map/psum | solution.py:43
  132.3 7.1 %psum.15 = f32[256]{0:T(256)S(1)} all-reduce(f32[256]{0:T(256)S(1)} %psum.14), channel_id=1, replica_groups=mesh['sp'=32,'tp_0'=4,'tp_1'=4] {'tp_1'}, use_global_device_ids=true, to_apply=%region_7.8 | all-reduce | flops 256 | bytes 2048 | tf_op jit(solution)/shard_map/psum | solution.py:43
  139.5 2.0 gather_fusion
  141.6 31.2 %all_to_all.20 = bf16[32,21,128]{2,1,0:T(8,128)(2,1)S(1)} all-to-all(bf16[32,21,128]{2,1,0:T(8,128)(2,1)S(1)} %reshape.594), channel_id=1, replica_groups=mesh['sp'=32,'tp_0'=4,'tp_1'=4] {'sp'}, dimensions={0} | all-to-all | bytes 344064 | tf_op jit(solution)/shard_map/all_to_all | solution.py:153
  172.8 14.0 %all_gather.10 = bf16[32,21,512]{2,0,1:T(8,128)(2,1)} all-gather(bf16[32,21,128]{2,0,1:T(8,128)(2,1)S(1)} %copy.48), channel_id=1, replica_groups=mesh['sp'=32,'tp_0'=4,'tp_1'=4] {'tp_1'}, dimensions={2}, use_global_device_ids=true | all-gather | bytes 860160 | tf_op jit(solution)/shard_map/all_gather | solution.py:50
  186.9 34.9 %all-gather.5.cloned.1.call-done = bf16[32,21,2048]{2,0,1:T(8,128)(2,1)} async-done(((bf16[32,21,512]{2,0,1:T(8,128)(2,1)}), bf16[32,21,2048]{2,0,1:T(8,128)(2,1)}) %all-gather.5.cloned.1.call-update) | async-done | bytes 2752528 | tf_op jit(solution)/shard_map/all_gather | solution.py:50
  221.7 3.5 %fusion.18 = f32[32,21,256]{2,0,1:T(8,128)} fusion(bf16[32,21,2048]{2,0,1:T(8,128)(2,1)} %all-gather.5.cloned.1.call-done, bf16[1,2048,256]{2,1,0:T(8,128)(2,1)S(1)} %copy-done.8), kind=kOutput, calls=%fused_computation.26 | convolution fusion | flops 704643072 | bytes 4489216 | tf_op jit(solution)/shard_map/scd,df->scf/dot_general | solution.py:155
  225.3 6.4 %fusion.7 = bf16[21,4,16,8,128]{4,3,2,1,0:T(8,128)(2,1)} fusion(bf16[1,256,2048]{2,1,0:T(8,128)(2,1)S(1)} %copy-done, bf16[32,21,2048]{2,0,1:T(8,128)(2,1)} %all-gather.5.cloned.1.call-done, bf16[1,2048,256]{2,1,0:T(8,128)(2,1)S(1)} %copy-done.9, f32[32,21,256]{2,0,1:T(8,128)} %fusion.18), kind=kOutput, calls=%fused_computation.15 | convolution fusion | flops 1411694592 | bytes 8290304 | tf_op jit(solution)/shard_map/scf,fd->scd/dot_general | solution.py:158
  231.7 2.2 copy.61
  234.0 39.4 %all_to_all.21 = bf16[16,32,21,128]{3,1,2,0:T(8,128)(2,1)} all-to-all(bf16[16,32,21,128]{3,1,2,0:T(8,128)(2,1)S(1)} %bitcast.107), channel_id=1, replica_groups=mesh['sp'=32,'tp_0'=4,'tp_1'=4] {'tp_0','tp_1'}, dimensions={0} | all-to-all | bytes 5505024 | tf_op jit(solution)/shard_map/all_to_all | solution.py:37
  273.4 2.2 reduce_sum.84
  276.4 14.6 %all-to-all-start.3 = ((bf16[32,21,128]{2,1,0:T(8,128)(2,1)}), bf16[32,21,128]{2,1,0:T(8,128)(2,1)S(1)}, u32[]{:S(2)}, u32[]{:S(2)}) async-start(bf16[32,21,128]{2,1,0:T(8,128)(2,1)} %copy.51), calls=%async_computation.3 | async-start | bytes 393216 | tf_op jit(solution)/shard_map/all_to_all | solution.py:162
  291.1 18.6 %all-to-all-done.3 = bf16[32,21,128]{2,1,0:T(8,128)(2,1)S(1)} async-done(((bf16[32,21,128]{2,1,0:T(8,128)(2,1)}), bf16[32,21,128]{2,1,0:T(8,128)(2,1)S(1)}, u32[]{:S(2)}, u32[]{:S(2)}) %all-to-all-start.3) | async-done | bytes 172064 | tf_op jit(solution)/shard_map/all_to_all | solution.py:162
  309.8 1.3 gather_fusion.1
  (67 shorter events, 9.1 us)
Async XLA Ops:
  6.5 218.8 %copy-start = (bf16[1,256,2048]{2,1,0:T(8,128)(2,1)S(1)}, bf16[1,256,2048]{2,1,0:T(8,128)(2,1)}, u32[]{:S(2)}) copy-start(bf16[1,256,2048]{2,1,0:T(8,128)(2,1)} %param.25) | copy-start | bytes 3145732
  6.5 81.6 %all-gather.3.cloned.1.call-start = ((), (), s32[]{:S(2)}) async-start(), calls=%async_computation.4 | async-start | bytes 2162688 | tf_op jit(solution)/shard_map/all_gather | solution.py:26
  12.1 78.9 %copy-start.4 = (s32[32,5]{0,1:T(8,128)}, s32[32,5]{0,1:T(8,128)S(1)}, u32[]{:S(2)}) copy-start(s32[32,5]{0,1:T(8,128)S(1)} %reduce-window.9) | copy-start | bytes 1924
  91.0 3.2 %copy-start.1 = (f32[8192,256]{1,0:T(8,128)}, f32[8192,256]{1,0:T(8,128)S(1)}, u32[]{:S(2)}) copy-start(f32[8192,256]{1,0:T(8,128)S(1)} %get-tuple-element.18) | copy-start | bytes 25165828
  94.2 1.2 copy-start.3
  101.2 7.9 %copy-start.5 = (s32[256,2]{0,1:T(2,128)S(1)}, s32[256,2]{0,1:T(2,128)}, u32[]{:S(2)}) copy-start(s32[256,2]{0,1:T(2,128)} %param.21) | copy-start | bytes 6148
  101.2 8.2 %slice-start = ((s32[32,5]{0,1:T(8,128)}), s32[32,4]{0,1:T(4,128)S(1)}, s32[]{:S(2)}) async-start(s32[32,5]{0,1:T(8,128)} %copy-done.4), calls=%async_computation.6 | async-start | bytes 4096 | tf_op jit(solution)/shard_map/slice.1
  101.2 24.4 %copy-start.2 = (bf16[256,128]{1,0:T(8,128)(2,1)S(1)}, bf16[256,128]{1,0:T(8,128)(2,1)}, u32[]{:S(2)}) copy-start(bf16[256,128]{1,0:T(8,128)(2,1)} %param.19) | copy-start | bytes 196612
  101.2 38.2 %copy-start.7 = (f32[128]{0:T(128)S(1)}, f32[128]{0:T(128)}, u32[]{:S(2)}) copy-start(f32[128]{0:T(128)} %param.20) | copy-start | bytes 1540
  102.5 23.0 %all-to-all-start = ((bf16[16,256,128]{2,1,0:T(8,128)(2,1)}), bf16[16,256,128]{2,1,0:T(8,128)(2,1)S(1)}, u32[]{:S(2)}, u32[]{:S(2)}) async-start(bf16[16,256,128]{2,1,0:T(8,128)(2,1)} %bitcast.106), calls=%async_computation | async-start | bytes 2097152 | tf_op jit(solution)/shard_map/all_to_all | solution.py:37
  109.0 112.7 %all-gather.5.cloned.1.call-start = ((), (), s32[]{:S(2)}) async-start(), calls=%async_computation.5 | async-start | bytes 3440640 | tf_op jit(solution)/shard_map/all_gather | solution.py:50
  112.0 109.7 %copy-start.8 = (bf16[1,2048,256]{2,1,0:T(8,128)(2,1)S(1)}, bf16[1,2048,256]{2,1,0:T(8,128)(2,1)}, u32[]{:S(2)}) copy-start(bf16[1,2048,256]{2,1,0:T(8,128)(2,1)} %param.23) | copy-start | bytes 3145732
  186.9 38.4 %copy-start.9 = (bf16[1,2048,256]{2,1,0:T(8,128)(2,1)S(1)}, bf16[1,2048,256]{2,1,0:T(8,128)(2,1)}, u32[]{:S(2)}) copy-start(bf16[1,2048,256]{2,1,0:T(8,128)(2,1)} %param.24) | copy-start | bytes 3145732
  273.4 17.5 %copy-start.6 = (f32[256,2]{0,1:T(2,128)S(1)}, f32[256,2]{0,1:T(2,128)}, u32[]{:S(2)}) copy-start(f32[256,2]{0,1:T(2,128)} %param.22) | copy-start | bytes 6148
  276.4 33.4 %all-to-all-start.3 = ((bf16[32,21,128]{2,1,0:T(8,128)(2,1)}), bf16[32,21,128]{2,1,0:T(8,128)(2,1)S(1)}, u32[]{:S(2)}, u32[]{:S(2)}) async-start(bf16[32,21,128]{2,1,0:T(8,128)(2,1)} %copy.51), calls=%async_computation.3 | async-start | bytes 393216 | tf_op jit(solution)/shard_map/all_to_all | solution.py:162
Sparse Core Ops, SparseCore 0:
  9.6 78.5 all-gather.2
  187.0 34.6 all-gather.4
where the time goes:
time: 320 us; the launch traced here: 319 us
  waiting for transfers between devices  141 us (44%)
  blocking collectives  98.3 us (31%)
  starting transfers between devices  21.1 us (7%)
  matrix products  18.6 us (6%)
  local copies, waits for them, and re-layouts  16.4 us (5%)
  between operations  13.8 us (4%)
  other arithmetic  9.64 us (3%)
    all_gather x1, waiting for transfers between devices, side_by_side(): lax.all_gather(both, axis, axis=dim, tiled=True)  74.3 us
    all_to_all x1, blocking collectives, sum_at_owner(): tiles = lax.all_to_all(cut_along(array, dim, peers), axis, 0, 0, tiled=True)  39.4 us
    all_gather x1, waiting for transfers between devices, gather_axes(): nearer = lax.all_gather(array, axes[-1], axis=dim, tiled=True)  34.9 us
    all_to_all x1, blocking collectives, shards(): lax.all_to_all(slot_rows, 'sp', split_axis=0, concat_axis=0, tiled=True)  31.2 us
    all_to_all x1, waiting for transfers between devices, shards(): lax.all_to_all(expert_rows, 'sp', split_axis=0, concat_axis=0, tiled=True)  18.6 us
    all_to_all x1, starting transfers between devices, shards(): lax.all_to_all(expert_rows, 'sp', split_axis=0, concat_axis=0, tiled=True)  14.6 us
    all_gather x1, blocking collectives, gather_axes(): nearer = lax.all_gather(array, axes[-1], axis=dim, tiled=True)  14 us
    psum x2, blocking collectives, by_axis(): array = lax.psum(array, axis)  13.7 us
  transfers between devices with their start and end apart: 4, of which 4 were waited for; matrix products, arithmetic and copies ran while one was open for 2% of the time, Pallas kernels for 0%

commit v1 on v0

v1 whole, which is shorter than its diff:
```python
import functools
import jax
import jax.numpy as jnp
import numpy as np
from jax import lax
from jax.experimental import pallas as pl
from jax.experimental.pallas import tpu as pltpu
from jax.sharding import Mesh
from jax.sharding import PartitionSpec as P

D = 2048
HQ = 16
KV = 4
E = 64
TOPK = 2
GRID_W = 64
CAP = 21
TOK = 256
LANES = 128
norm_eps = 1e-06
rope_base = 10000.0
MESH = pl.DeviceIdType.MESH


def rope_tables(n_rows):
    quarter = E // 4
    freq = (rope_base ** (-np.arange(quarter, dtype=np.float32) / quarter)).astype(np.float32)
    out = []
    for count, lo in ((n_rows, 0), (GRID_W, E // 2)):
        ang = np.arange(count, dtype=np.float32)[:, None] * freq[None, :]
        cos = np.zeros((count, LANES), np.float32)
        sin = np.zeros((count, LANES), np.float32)
        c, s = np.cos(ang), np.sin(ang)
        cos[:, lo : lo + quarter] = c
        cos[:, lo + quarter : lo + 2 * quarter] = c
        sin[:, lo : lo + quarter] = -s
        sin[:, lo + quarter : lo + 2 * quarter] = s
        if lo:
            cos[:, E:] = 1.0
        out += [cos, sin]
    return out


def attention_kernel(nz, tp_of, q_ref, k_ref, v_ref, qg_ref, kg_ref, rc_ref, rs_ref, cc_ref, cs_ref,
                     out_ref, kv, qt, q128, gains, cos_t, sin_t, m_ref, l_ref, acc,
                     send, recv, dsend, drecv):
    sp = lax.axis_index("sp")
    head = tp_of() // (HQ // KV)
    core = lax.rem(sp, 2)
    up = lax.rem(sp + 2, 2 * nz)
    down = lax.rem(sp + 2 * nz - 2, 2 * nz)
    partner = sp + 1 - 2 * core
    half = nz // 2

    barrier = pltpu.get_barrier_semaphore()
    for other in (up, down, partner):
        pl.semaphore_signal(barrier, inc=1, device_id={"sp": other}, device_id_type=MESH)

    lane = lax.broadcasted_iota(jnp.int32, (TOK, LANES), 1)
    low = lane < E
    rows_per = TOK // GRID_W
    for g in range(rows_per):
        at = pl.ds(g * GRID_W, GRID_W)
        cos_t[at, :] = cc_ref[...] + rc_ref[pl.ds(sp * rows_per + g, 1), :]
        sin_t[at, :] = cs_ref[...] + rs_ref[pl.ds(sp * rows_per + g, 1), :]
    gains[...] = jnp.ones_like(gains)
    gains[0:1, 0:E] = qg_ref[...]
    gains[1:2, 0:E] = kg_ref[...]

    def turned(x, gain):
        sq = jnp.where(low, x * x, 0.0)
        mean_sq = jnp.sum(sq, axis=1, keepdims=True) / E
        x = jnp.where(low, x * lax.rsqrt(mean_sq + norm_eps) * gain, x)
        swapped = jnp.where(
            lax.rem(lane, 32) < 16, pltpu.roll(x, LANES - 16, 1), pltpu.roll(x, 16, 1)
        )
        return x * cos_t[...] + swapped * sin_t[...]

    def tile_of(ref):
        return jnp.where(
            head >= 2, ref[:, LANES : 2 * LANES].astype(jnp.float32), ref[:, 0:LANES].astype(jnp.float32)
        )

    odd = lax.rem(head, 2) == 1
    kt = tile_of(k_ref)
    vt = tile_of(v_ref)
    k_lo = jnp.where(odd, pltpu.roll(kt, E, 1), kt)
    v_hi = jnp.where(odd, vt, pltpu.roll(vt, E, 1))
    kv[0, 0:TOK, :] = turned(jnp.where(low, k_lo, v_hi), gains[1:2, :]).astype(jnp.bfloat16)

    pl.semaphore_wait(barrier, 3)

    def unit(s, d):
        return 2 * s - 1 + d

    HB = TOK // 2

    def hop(s, d, h, src_u, dst_u):
        return pltpu.make_async_remote_copy(
            src_ref=kv.at[src_u, pl.ds(h * HB, HB)],
            dst_ref=kv.at[dst_u, pl.ds(h * HB, HB)],
            send_sem=send.at[s, d, h],
            recv_sem=recv.at[s, d, h],
            device_id={"sp": up if d == 0 else down},
            device_id_type=MESH,
        )

    def across(u):
        return pltpu.make_async_remote_copy(
            src_ref=kv.at[u, pl.ds(0, TOK)],
            dst_ref=kv.at[u, pl.ds(TOK, TOK)],
            send_sem=dsend.at[u],
            recv_sem=drecv.at[u],
            device_id={"sp": partner},
            device_id_type=MESH,
        )

    last = 2 * half - 1
    for h in range(2):
        for d in range(2):
            hop(1, d, h, 0, unit(1, d)).start()
    across(0).start()

    q128[...] = jnp.zeros_like(q128)
    q128[:, 0:E] = q_ref[...].astype(jnp.float32)
    q_rot = turned(q128[...], gains[0:1, :]) * (E ** -0.5)
    qt[...] = q_rot.T.astype(jnp.bfloat16)
    m_ref[...] = jnp.full_like(m_ref, -1e30)
    l_ref[...] = jnp.zeros_like(l_ref)
    acc[...] = jnp.zeros_like(acc)

    def attend(u):
        block = kv[u]
        s = jnp.dot(block, qt[...], preferred_element_type=jnp.float32)
        m_old = m_ref[...]
        m_new = jnp.maximum(m_old, jnp.max(s, axis=0, keepdims=True))
        alpha = jnp.exp(m_old - m_new)
        p = jnp.exp(s - m_new)
        l_ref[...] = l_ref[...] * alpha + jnp.sum(p, axis=0, keepdims=True)
        acc[...] = acc[...] * alpha + lax.dot_general(
            block, p.astype(jnp.bfloat16), (((0,), (0,)), ((), ())), preferred_element_type=jnp.float32
        )
        m_ref[...] = m_new

    def arrive(s, forward):
        for h in range(2):
            for d in range(2):
                hop(s, d, h, 0, unit(s, d)).wait_recv()
                forward(d, h)
        for d in range(2):
            across(unit(s, d)).start()

    def step(s, carry):
        def forward(d, h):
            hop(s + 1, d, h, unit(s, d), unit(s + 1, d)).start()

        arrive(s, forward)

        @pl.when(s == 1)
        def _():
            across(0).wait_recv()
            attend(0)

        @pl.when(s > 1)
        def _():
            for d in range(2):
                u = unit(s - 1, d)
                across(u).wait_recv()
                attend(u)

        return carry

    lax.fori_loop(1, half - 1, step, 0)

    def forward_last(d, h):
        if d == h:
            hop(half, d, h, unit(half - 1, d), last).start()

    arrive(half - 1, forward_last)
    for d in range(2):
        u = unit(half - 2, d)
        across(u).wait_recv()
        attend(u)
    for d in range(2):
        hop(half, d, d, 0, last).wait_recv()
    across(last).start()
    for d in range(2):
        u = unit(half - 1, d)
        across(u).wait_recv()
        attend(u)
    across(last).wait_recv()
    attend(last)
    out_ref[...] = (acc[E:, :] / l_ref[...]).astype(jnp.bfloat16)

    def drain(s, carry):
        for h in range(2):
            for d in range(2):
                hop(s, d, h, 0, unit(s, d)).wait_send()
        return carry

    lax.fori_loop(1, half, drain, 0)
    for d in range(2):
        hop(half, d, d, 0, last).wait_send()

    def drain_across(u, carry):
        across(u).wait_send()
        return carry

    lax.fori_loop(0, last + 1, drain_across, 0)


def attention(nz, tp_of, query_heads, key_heads, value_heads, q_gain, k_gain):
    tables = [jnp.asarray(t) for t in rope_tables(nz * 2 * TOK // GRID_W)]
    units = nz
    vmem = pl.BlockSpec(memory_space=pltpu.VMEM)
    return pl.pallas_call(
        functools.partial(attention_kernel, nz, tp_of),
        out_shape=jax.ShapeDtypeStruct((E, TOK), jnp.bfloat16),
        in_specs=[vmem] * 9,
        out_specs=vmem,
        scratch_shapes=[
            pltpu.VMEM((units, 2 * TOK, LANES), jnp.bfloat16),
            pltpu.VMEM((LANES, TOK), jnp.bfloat16),
            pltpu.VMEM((TOK, LANES), jnp.float32),
            pltpu.VMEM((8, LANES), jnp.float32),
            pltpu.VMEM((TOK, LANES), jnp.float32),
            pltpu.VMEM((TOK, LANES), jnp.float32),
            pltpu.VMEM((1, TOK), jnp.float32),
            pltpu.VMEM((1, TOK), jnp.float32),
            pltpu.VMEM((LANES, TOK), jnp.float32),
            pltpu.SemaphoreType.DMA((nz // 2 + 1, 2, 2)),
            pltpu.SemaphoreType.DMA((nz // 2 + 1, 2, 2)),
            pltpu.SemaphoreType.DMA((units,)),
            pltpu.SemaphoreType.DMA((units,)),
        ],
        compiler_params=pltpu.CompilerParams(collective_id=0, has_side_effects=True),
        cost_estimate=pl.CostEstimate(flops=10**9, bytes_accessed=2 * 10**6, transcendentals=0),
    )(query_heads, key_heads, value_heads, q_gain.reshape(1, E), k_gain.reshape(1, E), *tables)


TP = ("tp_0", "tp_1")


def cut_along(array, dim, peers):
    dims = array.shape
    tiles = array.reshape(*dims[:dim], peers, dims[dim] // peers, *dims[dim + 1 :])
    return jnp.moveaxis(tiles, dim, 0)


def sum_at_owner(array, axis, dim):
    peers = lax.axis_size(axis)
    tiles = lax.all_to_all(cut_along(array, dim, peers), axis, 0, 0, tiled=True)
    return jnp.sum(tiles.astype(jnp.float32), axis=0)


def by_axis(array, axes):
    for axis in axes:
        array = lax.psum(array, axis)
    return array


def gather_axes(array, axes, dim):
    if not axes:
        return array
    nearer = lax.all_gather(array, axes[-1], axis=dim, tiled=True)
    return gather_axes(nearer, axes[:-1], dim)


def shards(
    query_heads,
    key_heads,
    value_heads,
    q_gain,
    k_gain,
    out_weight,
    residual,
    norm_gain,
    routes,
    route_weights,
    w_gate,
    w_up,
    w_down,
):
    tok_rows = query_heads.shape[0]
    tok_rows = query_heads.shape[0]
    nz = lax.axis_size("sp") // 2
    attended_t = attention(nz, lambda: lax.axis_index(TP), query_heads, key_heads, value_heads, q_gain, k_gain)
    attended = attended_t.T
    partial_value = jnp.dot(attended, out_weight, preferred_element_type=jnp.float32).astype(
        jnp.bfloat16
    )
    attn_out = sum_at_owner(partial_value, TP, 1)
    after_attn = residual.astype(jnp.float32) + attn_out
    square_sum = by_axis(jnp.sum(after_attn * after_attn, axis=1), TP)
    normed = (after_attn * lax.rsqrt(square_sum / D + norm_eps)[:, None] * norm_gain).astype(
        jnp.bfloat16
    )
    experts_n = lax.axis_size("sp")
    capacity = 5 * tok_rows * TOPK // (4 * experts_n) + 1
    assign = routes.reshape(tok_rows * TOPK)
    onehot = (assign[:, None] == jnp.arange(experts_n, dtype=jnp.int32)[None, :]).astype(jnp.int32)
    before = jnp.cumsum(onehot, axis=0) - onehot
    slot_rank = jnp.sum(before * onehot, axis=1)
    slot_index = assign * capacity + slot_rank
    token_local = jnp.arange(tok_rows * TOPK, dtype=jnp.int32) // TOPK
    slot_token = (
        jnp.full((experts_n * capacity,), tok_rows, jnp.int32).at[slot_index].set(token_local)
    )
    gate_w = w_gate[0]
    up_w = w_up[0]
    down_w = w_down[0]
    padded = jnp.concatenate([normed, jnp.zeros((1, normed.shape[1]), jnp.bfloat16)], axis=0)
    slot_rows = padded[slot_token].reshape(experts_n, capacity, normed.shape[1])
    block_rows = gather_axes(
        lax.all_to_all(slot_rows, "sp", split_axis=0, concat_axis=0, tiled=True), TP, 2
    )
    gate_next = jnp.einsum("scd,df->scf", block_rows, gate_w, preferred_element_type=jnp.float32)
    up_next = jnp.einsum("scd,df->scf", block_rows, up_w, preferred_element_type=jnp.float32)
    activated = (jax.nn.silu(gate_next) * up_next).astype(jnp.bfloat16)
    partials = jnp.einsum(
        "scf,fd->scd", activated, down_w, preferred_element_type=jnp.float32
    ).astype(jnp.bfloat16)
    expert_rows = sum_at_owner(partials, TP, 2).astype(jnp.bfloat16)
    returned_rows = lax.all_to_all(expert_rows, "sp", split_axis=0, concat_axis=0, tiled=True)
    columns = returned_rows.shape[2]
    picked = returned_rows.reshape(experts_n * capacity, columns)[slot_index].astype(jnp.float32)
    picked = picked.reshape(tok_rows, TOPK, columns)
    expert_mix = jnp.sum(picked * route_weights[:, :, None], axis=1)
    return (after_attn + expert_mix).astype(jnp.bfloat16)


def solution(mesh):
    finer = Mesh(mesh.devices.reshape(mesh.shape["sp"], 4, 4), ("sp", "tp_0", "tp_1"))
    in_specs = (
        P("sp", TP),
        P("sp", None),
        P("sp", None),
        P(),
        P(),
        P(TP, None),
        P("sp", TP),
        P(TP),
        P("sp", None),
        P("sp", None),
        P("sp", None, TP),
        P("sp", None, TP),
        P("sp", TP, None),
    )
    out_specs = P("sp", TP)
    return jax.shard_map(
        shards, mesh=finer, in_specs=in_specs, out_specs=out_specs, check_vma=False
    )
```

time: 320 us -> 270 us (0.84)
  waiting for transfers between devices: 141 us -> 65.1 us
  Pallas kernels: 0 us -> 41.8 us
  matrix products: 18.6 us -> 11.2 us
  other arithmetic: 9.64 us -> 4.99 us
  local copies, waits for them, and re-layouts: 16.4 us -> 12.9 us
    all_gather x1 -> x0, waiting for transfers between devices: 74.3 us -> none  [side_by_side(): lax.all_gather(both, axis, axis=dim, tiled=True)]
    pallas_call x0 -> x1, Pallas kernels: none -> 41.8 us  [attention(): pl.pallas_call(functools.partial(attention_kernel, nz, tp_of), out_shape=...]
    dot_general x1, matrix products: 5.79 us -> 1.21 us  [shards(): jnp.dot(attended, out_weight, preferred_element_type=jnp.float32)]
  transfers between devices with their start and end apart: 4 -> 3, of which waited for: 4 -> 3; matrix products, arithmetic and copies ran while one was open for 2% -> 2% of each run, Pallas kernels for 0% -> 0%
where the time goes in v1:
time: 270 us; the launch traced here: 269 us
  blocking collectives  98.4 us (36%)
  waiting for transfers between devices  65.1 us (24%)
  Pallas kernels  41.8 us (15%)
  starting transfers between devices  21.5 us (8%)
  between operations  13.6 us (5%)
  local copies, waits for them, and re-layouts  12.9 us (5%)
  matrix products  11.2 us (4%)
  other arithmetic  4.99 us (2%)
    pallas_call x1, Pallas kernels, attention(): pl.pallas_call(functools.partial(attention_kernel, nz, tp_of), out_shape=...  41.8 us
    all_to_all x1, blocking collectives, sum_at_owner(): tiles = lax.all_to_all(cut_along(array, dim, peers), axis, 0, 0, tiled=True)  39.4 us
    all_gather x1, waiting for transfers between devices, gather_axes(): nearer = lax.all_gather(array, axes[-1], axis=dim, tiled=True)  34.9 us
    all_to_all x1, blocking collectives, shards(): lax.all_to_all(slot_rows, 'sp', split_axis=0, concat_axis=0, tiled=True)  31.8 us
    all_to_all x1, waiting for transfers between devices, shards(): lax.all_to_all(expert_rows, 'sp', split_axis=0, concat_axis=0, tiled=True)  18.6 us
    all_to_all x1, starting transfers between devices, shards(): lax.all_to_all(expert_rows, 'sp', split_axis=0, concat_axis=0, tiled=True)  14.6 us
    all_gather x1, blocking collectives, gather_axes(): nearer = lax.all_gather(array, axes[-1], axis=dim, tiled=True)  13.8 us
    psum x2, blocking collectives, by_axis(): array = lax.psum(array, axis)  13.3 us
  transfers between devices with their start and end apart: 3, of which 3 were waited for; matrix products, arithmetic and copies ran while one was open for 2% of the time, Pallas kernels for 0%

profile of v1, /device:TPU:1, one launch (start us, length us, event | category | flops | bytes accessed | tf_op | source)
XLA Modules:
  0.0 269.5 jit_solution(10975391566994843763)
XLA Ops:
  6.5 1.6 copy.38.q_ref
  8.1 41.8 %shard_map.163 = bf16[64,256]{1,0:T(8,128)(2,1)} custom-call(bf16[256,64]{1,0:T(8,128)(2,1)} %copy.38.q_ref, bf16[256,256]{1,0:T(8,128)(2,1)} %k_ref.1, bf16[256,256]{1,0:T(8,128)(2,1)} %v_ref.1, f32[1,64]{1,0:T(1,128)} %bitcast.64, f32[1,64]{1,0:T(1,128)} %bitcast.65, f32[128,128]{1,0:T(8,128)} %constant.52.clone.rc_ref, f32[128,128]{1,0:T(8,128)} %constant.53.clone.rs_ref, ...), custom_call_target="tpu_custom_call" | custom-call | flops 1000000000 | bytes 2000000 | tf_op jit(solution)/shard_map/pallas_call | solution.py:216
  50.0 1.2 fusion.1
  51.2 1.3 copy.57
  52.5 6.9 %all-to-all-start = ((bf16[16,256,128]{2,1,0:T(8,128)(2,1)}), bf16[16,256,128]{2,1,0:T(8,128)(2,1)S(1)}, u32[]{:S(2)}, u32[]{:S(2)}) async-start(bf16[16,256,128]{2,1,0:T(8,128)(2,1)} %bitcast.58), calls=%async_computation | async-start | bytes 2097152 | tf_op jit(solution)/shard_map/all_to_all | solution.py:252
  59.9 1.2 reduce-window.6
  61.8 2.4 scatter_custom_fusion
  64.3 11.6 %all-to-all-done = bf16[16,256,128]{2,1,0:T(8,128)(2,1)S(1)} async-done(((bf16[16,256,128]{2,1,0:T(8,128)(2,1)}), bf16[16,256,128]{2,1,0:T(8,128)(2,1)S(1)}, u32[]{:S(2)}, u32[]{:S(2)}) %all-to-all-start) | async-done | bytes 1048608 | tf_op jit(solution)/shard_map/all_to_all | solution.py:252
  76.1 6.6 %psum.14 = f32[256]{0:T(256)S(1)} all-reduce(f32[256]{0:T(256)S(1)} %multiply_reduce_fusion), channel_id=1, replica_groups=mesh['sp'=32,'tp_0'=4,'tp_1'=4] {'tp_0'}, use_global_device_ids=true, to_apply=%region_2.0 | all-reduce | flops 256 | bytes 2048 | tf_op jit(solution)/shard_map/psum | solution.py:258
  82.6 6.8 %psum.15 = f32[256]{0:T(256)S(1)} all-reduce(f32[256]{0:T(256)S(1)} %psum.14), channel_id=1, replica_groups=mesh['sp'=32,'tp_0'=4,'tp_1'=4] {'tp_1'}, use_global_device_ids=true, to_apply=%region_3.0 | all-reduce | flops 256 | bytes 2048 | tf_op jit(solution)/shard_map/psum | solution.py:258
  89.5 2.0 gather_fusion
  91.6 31.8 %all_to_all.20 = bf16[32,21,128]{2,1,0:T(8,128)(2,1)S(1)} all-to-all(bf16[32,21,128]{2,1,0:T(8,128)(2,1)S(1)} %reshape.75), channel_id=1, replica_groups=mesh['sp'=32,'tp_0'=4,'tp_1'=4] {'sp'}, dimensions={0} | all-to-all | bytes 344064 | tf_op jit(solution)/shard_map/all_to_all | solution.py:315
  123.5 13.8 %all_gather.6 = bf16[32,21,512]{2,0,1:T(8,128)(2,1)} all-gather(bf16[32,21,128]{2,0,1:T(8,128)(2,1)S(1)} %copy.44), channel_id=1, replica_groups=mesh['sp'=32,'tp_0'=4,'tp_1'=4] {'tp_1'}, dimensions={2}, use_global_device_ids=true | all-gather | bytes 860160 | tf_op jit(solution)/shard_map/all_gather | solution.py:265
  137.3 34.9 %all-gather.2.cloned.1.call-done = bf16[32,21,2048]{2,0,1:T(8,128)(2,1)} async-done(((bf16[32,21,512]{2,0,1:T(8,128)(2,1)}), bf16[32,21,2048]{2,0,1:T(8,128)(2,1)}) %all-gather.2.cloned.1.call-update) | async-done | bytes 2752528 | tf_op jit(solution)/shard_map/all_gather | solution.py:265
  172.2 3.5 %fusion.5 = f32[32,21,256]{2,0,1:T(8,128)} fusion(bf16[32,21,2048]{2,0,1:T(8,128)(2,1)} %all-gather.2.cloned.1.call-done, bf16[1,2048,256]{2,1,0:T(8,128)(2,1)S(1)} %copy-done.6), kind=kOutput, calls=%fused_computation.14 | convolution fusion | flops 704643072 | bytes 4489216 | tf_op jit(solution)/shard_map/scd,df->scf/dot_general | solution.py:317
  175.7 6.4 %fusion = bf16[21,4,16,8,128]{4,3,2,1,0:T(8,128)(2,1)} fusion(bf16[1,256,2048]{2,1,0:T(8,128)(2,1)S(1)} %copy-done, bf16[32,21,2048]{2,0,1:T(8,128)(2,1)} %all-gather.2.cloned.1.call-done, bf16[1,2048,256]{2,1,0:T(8,128)(2,1)S(1)} %copy-done.7, f32[32,21,256]{2,0,1:T(8,128)} %fusion.5), kind=kOutput, calls=%fused_computation.7 | convolution fusion | flops 1411694592 | bytes 8290304 | tf_op jit(solution)/shard_map/scf,fd->scd/dot_general | solution.py:320
  182.2 2.2 copy.56
  184.4 39.4 %all_to_all.21 = bf16[16,32,21,128]{3,1,2,0:T(8,128)(2,1)} all-to-all(bf16[16,32,21,128]{3,1,2,0:T(8,128)(2,1)S(1)} %bitcast.59), channel_id=1, replica_groups=mesh['sp'=32,'tp_0'=4,'tp_1'=4] {'tp_0','tp_1'}, dimensions={0} | all-to-all | bytes 5505024 | tf_op jit(solution)/shard_map/all_to_all | solution.py:252
  223.8 2.2 reduce_sum.54
  226.1 0.7 copy.47
  226.8 14.6 %all-to-all-start.3 = ((bf16[32,21,128]{2,1,0:T(8,128)(2,1)}), bf16[32,21,128]{2,1,0:T(8,128)(2,1)S(1)}, u32[]{:S(2)}, u32[]{:S(2)}) async-start(bf16[32,21,128]{2,1,0:T(8,128)(2,1)} %copy.47), calls=%async_computation.3 | async-start | bytes 393216 | tf_op jit(solution)/shard_map/all_to_all | solution.py:324
  241.5 18.6 %all-to-all-done.3 = bf16[32,21,128]{2,1,0:T(8,128)(2,1)S(1)} async-done(((bf16[32,21,128]{2,1,0:T(8,128)(2,1)}), bf16[32,21,128]{2,1,0:T(8,128)(2,1)S(1)}, u32[]{:S(2)}, u32[]{:S(2)}) %all-to-all-start.3) | async-done | bytes 172064 | tf_op jit(solution)/shard_map/all_to_all | solution.py:324
  260.2 1.3 gather_fusion.1
  262.0 0.7 add_convert_fusion
  (44 shorter events, 2.3 us)
Async XLA Ops:
  6.5 169.2 %copy-start = (bf16[1,256,2048]{2,1,0:T(8,128)(2,1)S(1)}, bf16[1,256,2048]{2,1,0:T(8,128)(2,1)}, u32[]{:S(2)}) copy-start(bf16[1,256,2048]{2,1,0:T(8,128)(2,1)} %param.29) | copy-start | bytes 3145732
  6.5 43.4 %copy-start.2 = (bf16[64,2048]{1,0:T(8,128)(2,1)S(1)}, bf16[64,2048]{1,0:T(8,128)(2,1)}, u32[]{:S(2)}) copy-start(bf16[64,2048]{1,0:T(8,128)(2,1)} %param.22) | copy-start | bytes 786436
  50.0 9.5 %copy-start.3 = (s32[256,2]{0,1:T(2,128)S(1)}, s32[256,2]{0,1:T(2,128)}, u32[]{:S(2)}) copy-start(s32[256,2]{0,1:T(2,128)} %param.25) | copy-start | bytes 6148
  51.2 24.7 %copy-start.1 = (bf16[256,128]{1,0:T(8,128)(2,1)S(1)}, bf16[256,128]{1,0:T(8,128)(2,1)}, u32[]{:S(2)}) copy-start(bf16[256,128]{1,0:T(8,128)(2,1)} %param.23) | copy-start | bytes 196612
  52.5 36.9 %copy-start.5 = (f32[128]{0:T(128)S(1)}, f32[128]{0:T(128)}, u32[]{:S(2)}) copy-start(f32[128]{0:T(128)} %param.24) | copy-start | bytes 1540
  52.5 23.3 %all-to-all-start = ((bf16[16,256,128]{2,1,0:T(8,128)(2,1)}), bf16[16,256,128]{2,1,0:T(8,128)(2,1)S(1)}, u32[]{:S(2)}, u32[]{:S(2)}) async-start(bf16[16,256,128]{2,1,0:T(8,128)(2,1)} %bitcast.58), calls=%async_computation | async-start | bytes 2097152 | tf_op jit(solution)/shard_map/all_to_all | solution.py:252
  59.4 112.8 %all-gather.2.cloned.1.call-start = ((), (), s32[]{:S(2)}) async-start(), calls=%async_computation.4 | async-start | bytes 3440640 | tf_op jit(solution)/shard_map/all_gather | solution.py:265
  64.2 107.9 %copy-start.6 = (bf16[1,2048,256]{2,1,0:T(8,128)(2,1)S(1)}, bf16[1,2048,256]{2,1,0:T(8,128)(2,1)}, u32[]{:S(2)}) copy-start(bf16[1,2048,256]{2,1,0:T(8,128)(2,1)} %param.27) | copy-start | bytes 3145732
  137.3 38.4 %copy-start.7 = (bf16[1,2048,256]{2,1,0:T(8,128)(2,1)S(1)}, bf16[1,2048,256]{2,1,0:T(8,128)(2,1)}, u32[]{:S(2)}) copy-start(bf16[1,2048,256]{2,1,0:T(8,128)(2,1)} %param.28) | copy-start | bytes 3145732
  223.8 17.5 %copy-start.4 = (f32[256,2]{0,1:T(2,128)S(1)}, f32[256,2]{0,1:T(2,128)}, u32[]{:S(2)}) copy-start(f32[256,2]{0,1:T(2,128)} %param.26) | copy-start | bytes 6148
  226.8 33.4 %all-to-all-start.3 = ((bf16[32,21,128]{2,1,0:T(8,128)(2,1)}), bf16[32,21,128]{2,1,0:T(8,128)(2,1)S(1)}, u32[]{:S(2)}, u32[]{:S(2)}) async-start(bf16[32,21,128]{2,1,0:T(8,128)(2,1)} %copy.47), calls=%async_computation.3 | async-start | bytes 393216 | tf_op jit(solution)/shard_map/all_to_all | solution.py:324
Sparse Core Ops, SparseCore 0:
  137.4 34.6 all-gather.1
